TPU v7x, 32 devices: a whole 2x2x4 slice. The times are simulated.
32 devices in a mesh: kv: 4 (over y, x), tp: 8 (over z, core).
Axes of the slice: x: 2, y: 2, z: 4, core: 2. Of those that a mesh axis runs over, the one named last changes fastest.
Arguments:
- residual: bfloat16 [128, 4096], P(None, ('kv', 'tp')), may hold values from -20 to 20
- mixer_gain: float32 [4096], P('kv'), may hold values from 0.1 to 1.9
- w_query: bfloat16 [4096, 4096], P('kv', 'tp'), may hold values from -0.09375 to 0.09375
- w_forget: bfloat16 [4096, 4096], P('kv', 'tp'), may hold values from -0.09375 to 0.09375
- w_input: bfloat16 [4096, 4096], P('kv', 'tp'), may hold values from -0.09375 to 0.09375
- w_outgate: bfloat16 [4096, 4096], P('kv', 'tp'), may hold values from -0.09375 to 0.09375
- lower_bound: float32 [4096], P('tp'), may hold values from 0.3 to 0.97
- state: float32 [128, 32, 128, 128], P('kv', 'tp'), may hold values from -6 to 6
- head_gain: float32 [128], replicated, may hold values from 0.1 to 1.9
- w_mix_out: bfloat16 [4096, 4096], P('tp', 'kv'), may hold values from -0.09375 to 0.09375
- ffn_gain: float32 [4096], P('kv'), may hold values from 0.1 to 1.9
- w_gate: bfloat16 [4096, 10752], P('kv', 'tp'), may hold values from -0.09375 to 0.09375
- w_up: bfloat16 [4096, 10752], P('kv', 'tp'), may hold values from -0.09375 to 0.09375
- w_down: bfloat16 [10752, 4096], P('tp', 'kv'), may hold values from -0.0625 to 0.0625
Outputs:
- layer_out: bfloat16 [128, 4096], P(None, ('kv', 'tp'))
- new_state: float32 [128, 32, 128, 128], P('kv', 'tp')
All inputs are finite; a program needn't handle non-finite values.
Results may differ from a plain program's by a relative error of at most 0.015.
Values may be sent and summed in bfloat16 or wider, within the bound.
No kernel may reach another device: no remote copies, remote signals or barrier semaphores. Data moves between devices by JAX's collectives and lax.ppermute only.
A program may use at most 64 MiB of HBM per device.

v0:
```python
import jax
import jax.numpy as jnp
from jax import lax
from jax.sharding import PartitionSpec as P

D = 4096
DK = 128
DV = 128
EPS = 1e-06


def project_row(weight, piece):
    return jnp.dot(piece, weight, preferred_element_type=jnp.float32)


def channel_mix(rows_in, ffn_gain, w_gate, w_up, w_down):
    rows_float = rows_in.astype(jnp.float32)
    squares = jnp.sum(rows_float * rows_float, axis=1)
    scaled = (rows_float * ffn_gain).astype(jnp.bfloat16)
    gate = jnp.dot(scaled, w_gate, preferred_element_type=jnp.float32)
    upper = jnp.dot(scaled, w_up, preferred_element_type=jnp.float32)
    whole_total = lax.psum(squares, "kv")
    gate, upper = (
        lax.psum(gate.astype(jnp.bfloat16), "kv").astype(jnp.float32),
        lax.psum(upper.astype(jnp.bfloat16), "kv").astype(jnp.float32),
    )
    inverse = lax.rsqrt(whole_total / D + EPS)[:, None]
    hidden = (jax.nn.silu(gate * inverse) * (upper * inverse)).astype(jnp.bfloat16)
    terms = jnp.dot(hidden, w_down, preferred_element_type=jnp.float32)
    summed = lax.psum_scatter(
        terms.astype(jnp.bfloat16), "tp", scatter_dimension=1, tiled=True
    ).astype(jnp.float32)
    width = summed.shape[1]
    own = lax.dynamic_slice_in_dim(rows_float, lax.axis_index("tp") * width, width, 1)
    return (own + summed).astype(jnp.bfloat16)


def body(
    residual,
    mixer_gain,
    w_query,
    w_forget,
    w_input,
    w_outgate,
    lower_bound,
    state,
    head_gain,
    w_mix_out,
    ffn_gain,
    w_gate,
    w_up,
    w_down,
):
    local_seqs, local_heads = (state.shape[0], state.shape[1])
    rows = lax.all_gather(residual, "tp", axis=1, tiled=True)
    rows_float = rows.astype(jnp.float32)
    squares = jnp.sum(rows_float * rows_float, axis=1)
    scaled = (rows_float * mixer_gain).astype(jnp.bfloat16)
    part_query = jnp.dot(scaled, w_query, preferred_element_type=jnp.float32)
    part_forget = jnp.dot(scaled, w_forget, preferred_element_type=jnp.float32)
    part_value = jnp.dot(scaled, w_input, preferred_element_type=jnp.float32)
    part_gate = jnp.dot(scaled, w_outgate, preferred_element_type=jnp.float32)
    whole_total = lax.psum(squares, "kv")
    total = lax.dynamic_slice_in_dim(whole_total, lax.axis_index("kv") * local_seqs, local_seqs)
    part_query, part_forget, part_value, part_gate = (
        lax.psum_scatter(part_query, "kv", scatter_dimension=0, tiled=True),
        lax.psum_scatter(part_forget, "kv", scatter_dimension=0, tiled=True),
        lax.psum_scatter(part_value, "kv", scatter_dimension=0, tiled=True),
        lax.psum_scatter(part_gate, "kv", scatter_dimension=0, tiled=True),
    )
    inverse = lax.rsqrt(total / D + EPS)[:, None]
    bound = lower_bound.reshape(local_heads, DK)
    forget_raw = (part_forget * inverse).reshape(local_seqs, local_heads, DK)
    forget = bound + (1.0 - bound) * jax.nn.sigmoid(forget_raw)
    keyvec = (1.0 - bound) * jax.nn.sigmoid(-forget_raw)
    query = jax.nn.silu((part_query * inverse).reshape(local_seqs, local_heads, DK))
    values = (part_value * inverse).reshape(local_seqs, local_heads, DV)
    updated = forget[..., None] * state + keyvec[..., None] * values[:, :, None, :]
    head_out = jnp.einsum("shc,shce->she", query, updated, precision=lax.Precision.HIGHEST)
    inv_head = lax.rsqrt(jnp.mean(head_out * head_out, axis=2, keepdims=True) + EPS)
    out_gate = jax.nn.silu((part_gate * inverse).reshape(local_seqs, local_heads, DV))
    normed = (
        (head_out * inv_head * head_gain * out_gate)
        .reshape(local_seqs, local_heads * DV)
        .astype(jnp.bfloat16)
    )
    terms = project_row(w_mix_out, lax.all_gather(normed, "kv", axis=0, tiled=True))
    mixed = lax.psum(terms, "tp")
    after_mix = (rows_float + mixed).astype(jnp.bfloat16)
    layer_out = channel_mix(after_mix, ffn_gain, w_gate, w_up, w_down)
    return (layer_out, updated)


def solution(mesh):
    in_specs = (
        P(None, ("kv", "tp")),
        P("kv"),
        P("kv", "tp"),
        P("kv", "tp"),
        P("kv", "tp"),
        P("kv", "tp"),
        P("tp"),
        P("kv", "tp", None, None),
        P(),
        P("tp", "kv"),
        P("kv"),
        P("kv", "tp"),
        P("kv", "tp"),
        P("tp", "kv"),
    )
    out_specs = (P(None, ("kv", "tp")), P("kv", "tp", None, None))
    return jax.shard_map(body, mesh=mesh, in_specs=in_specs, out_specs=out_specs, check_vma=False)
```

profile of v0, /device:TPU:0, one launch (start us, length us, event | category | flops | bytes accessed | tf_op | source)
XLA Modules:
  0.0 312.9 jit_solution(12020792351462122957)
XLA Ops:
  7.2 0.0 copy-start
  7.2 0.0 copy-start.4
  7.2 0.0 reduce-scatter.10.cloned.1.call-start
  7.2 15.1 %all_gather.6 = bf16[128,1024]{1,0:T(8,128)(2,1)S(1)} all-gather(bf16[128,128]{1,0:T(8,128)(2,1)} %param.14), channel_id=1, replica_groups=mesh['kv'=4,'tp'=8] {'tp'}, dimensions={1}, use_global_device_ids=true | all-gather | bytes 294912 | tf_op jit(solution)/shard_map/all_gather | solution.py:55
  22.4 2.3 fusion.10
  24.6 0.0 reduce-scatter.10.cloned.1.call-update
  24.7 0.0 reduce-scatter.12.cloned.1.call-start
  24.7 2.2 fusion.8
  27.0 0.0 reduce-scatter.12.cloned.1.call-update
  27.0 0.0 reduce-scatter.14.cloned.1.call-start
  27.0 2.3 fusion.6
  29.3 0.0 reduce-scatter.14.cloned.1.call-update
  29.3 0.0 reduce-scatter.8.cloned.1.call-start
  29.4 2.3 fusion.12
  31.6 0.0 reduce-scatter.8.cloned.1.call-update
  31.7 0.0 all-reduce.4.cloned.1.call-start
  31.7 0.1 fusion.1
  31.8 9.9 %psum.35 = f32[128]{0:T(128)S(1)} all-reduce(f32[128]{0:T(128)S(1)} %fusion.1), channel_id=1, replica_groups=mesh['kv'=4,'tp'=8] {'kv'}, use_global_device_ids=true, to_apply=%region_2.0 | all-reduce | flops 128 | bytes 1024 | tf_op jit(solution)/shard_map/psum | solution.py:63
  41.8 0.1 add_rsqrt_fusion.2
  41.8 0.7 broadcast_subtract_fusion
  42.5 6.5 %reduce-scatter.10.cloned.1.call-done = f32[32,512]{1,0:T(8,128)} async-done(((f32[128,512]{1,0:T(8,128)}), f32[32,512]{1,0:T(8,128)}) %reduce-scatter.10.cloned.1.call-update) | async-done | bytes 65552 | tf_op jit(solution)/shard_map/reduce_scatter | solution.py:67
  49.0 27.1 %reduce-scatter.12.cloned.1.call-done = f32[32,512]{1,0:T(8,128)} async-done(((f32[128,512]{1,0:T(8,128)}), f32[32,512]{1,0:T(8,128)}) %reduce-scatter.12.cloned.1.call-update) | async-done | bytes 65552 | tf_op jit(solution)/shard_map/reduce_scatter | solution.py:68
  76.1 27.2 %reduce-scatter.14.cloned.1.call-done = f32[32,512]{1,0:T(8,128)} async-done(((f32[128,512]{1,0:T(8,128)}), f32[32,512]{1,0:T(8,128)}) %reduce-scatter.14.cloned.1.call-update) | async-done | bytes 65552 | tf_op jit(solution)/shard_map/reduce_scatter | solution.py:69
  103.3 27.0 %reduce-scatter.8.cloned.1.call-done = f32[32,512]{1,0:T(8,128)} async-done(((f32[128,512]{1,0:T(8,128)}), f32[32,512]{1,0:T(8,128)}) %reduce-scatter.8.cloned.1.call-update) | async-done | bytes 65552 | tf_op jit(solution)/shard_map/reduce_scatter | solution.py:66
  130.3 1.0 add_divide_fusion.1
  131.6 0.0 copy-done.4
  131.6 8.2 %multiply_add_fusion = f32[32,4,128,128]{3,2,1,0:T(8,128)S(1)} fusion(f32[32,4,128,128]{3,2,1,0:T(8,128)} %param.21, f32[32,4,128]{2,1,0:T(4,128)S(1)} %mul.164, f32[32,4,128]{2,1,0:T(4,128)S(1)} %bitcast.35, f32[32,4,128]{2,1,0:T(4,128)S(1)} %bitcast.34), kind=kLoop, calls=%fused_computation | loop fusion | flops 6291456 | bytes 16973824 | tf_op jit(solution)/shard_map/add | solution.py:78
  139.8 0.0 copy-start.1
  139.8 0.0 copy-start.5
  139.9 0.0 copy-start.2
  139.9 0.0 copy-start.3
  139.9 3.4 %copy-done.1 = f32[32,4,128,128]{3,2,1,0:T(8,128)} copy-done((f32[32,4,128,128]{3,2,1,0:T(8,128)}, f32[32,4,128,128]{3,2,1,0:T(8,128)S(1)}, u32[]{:S(2)}) %copy-start.1) | copy-done | bytes 8388632
  143.2 7.2 %fusion.18 = f32[32,4,1,128]{3,2,1,0:T(1,128)S(1)} fusion(f32[32,4,128,1]{2,3,1,0:T(1,128)S(1)} %bitcast.33, f32[32,4,128,128]{3,2,1,0:T(8,128)S(1)} %multiply_add_fusion), kind=kOutput, calls=%fused_computation.39 | convolution fusion | flops 25165824 | bytes 8519680 | tf_op jit(solution)/shard_map/shc,shce->she/dot_general | solution.py:79
  150.5 0.1 multiply_reduce_fusion.1
  150.6 0.0 copy-done.5
  150.6 0.1 fusion.15
  150.8 8.5 %all_gather.7 = bf16[128,512]{1,0:T(8,128)(2,1)S(1)} all-gather(bf16[32,512]{1,0:T(8,128)(2,1)S(1)} %bitcast.38), channel_id=1, replica_groups=mesh['kv'=4,'tp'=8] {'kv'}, dimensions={0}, use_global_device_ids=true | all-gather | bytes 163840 | tf_op jit(solution)/shard_map/all_gather | solution.py:87
  159.2 0.0 copy-done.2
  159.2 1.1 fusion.19
  160.4 0.0 all-reduce.4.cloned.1.call-update
  160.4 0.0 all-reduce.6.cloned.1.call-start
  160.4 56.7 %all-reduce.4.cloned.1.call-done = f32[128,1024]{1,0:T(8,128)} async-done(((f32[128,1024]{1,0:T(8,128)}), f32[128,1024]{1,0:T(8,128)}) %all-reduce.4.cloned.1.call-update) | async-done | bytes 524304 | tf_op jit(solution)/shard_map/psum | solution.py:88
  217.1 1.2 multiply_reduce_fusion
  218.3 0.0 copy-done
  218.3 0.0 copy-done.3
  218.3 1.6 convolution_convert_fusion
  219.9 3.4 %convolution_convert_fusion.1 = bf16[128,1344]{0,1:T(8,128)(2,1)} fusion(bf16[1024,1344]{0,1:T(8,128)(2,1)} %param.25, f32[128,1024]{1,0:T(8,128)S(1)} %get-tuple-element.5, f32[1024]{0:T(1024)S(1)} %copy-done.3), kind=kOutput, calls=%fused_computation.2 | convolution fusion | flops 352755712 | bytes 3624960 | tf_op jit(solution)/shard_map/dot_general | solution.py:20
  223.3 0.0 all-reduce.6.cloned.1.call-update
  223.4 0.0 reduce-scatter.16.cloned.1.call-start
  223.4 10.2 %psum.38 = f32[128]{0:T(128)S(1)} all-reduce(f32[128]{0:T(128)S(1)} %get-tuple-element.4), channel_id=1, replica_groups=mesh['kv'=4,'tp'=8] {'kv'}, use_global_device_ids=true, to_apply=%region_10.11 | all-reduce | flops 128 | bytes 1024 | tf_op jit(solution)/shard_map/psum | solution.py:22
  233.6 36.4 %all-reduce.6.cloned.1.call-done = (bf16[128,1344]{0,1:T(8,128)(2,1)}, bf16[128,1344]{0,1:T(8,128)(2,1)}) async-done(((bf16[128,1344]{0,1:T(8,128)(2,1)}, bf16[128,1344]{0,1:T(8,128)(2,1)}), (bf16[128,1344]{0,1:T(8,128)(2,1)}, bf16[128,1344]{0,1:T(8,128)(2,1)})) %all-reduce.6.cloned.1.call-update) | async-done | bytes 688144 | tf_op jit(solution)/shard_map/psum | solution.py:25
  270.0 2.8 convolution_convert_fusion.2
  272.7 0.8 copy.18
  273.6 0.0 reduce-scatter.16.cloned.1.call-update
  273.6 31.0 %reduce-scatter.16.cloned.1.call-done = bf16[128,128]{1,0:T(8,128)(2,1)} async-done(((bf16[1024,128]{1,0:T(8,128)(2,1)}), bf16[128,128]{1,0:T(8,128)(2,1)}) %reduce-scatter.16.cloned.1.call-update) | async-done | bytes 32784
  304.5 0.9 copy.19
  305.4 0.6 add_convert_fusion
  (12 shorter events, 0.2 us)
Async XLA Ops:
  7.2 211.1 %copy-start = (bf16[1024,1344]{0,1:T(8,128)(2,1)S(1)}, bf16[1024,1344]{0,1:T(8,128)(2,1)}, u32[]{:S(2)}) copy-start(bf16[1024,1344]{0,1:T(8,128)(2,1)} %param.26) | copy-start | bytes 8257540
  7.2 124.4 %copy-start.4 = (f32[512]{0:T(512)S(1)}, f32[512]{0:T(512)}, u32[]{:S(2)}) copy-start(f32[512]{0:T(512)} %param.20) | copy-start | bytes 6148
  7.2 41.8 %reduce-scatter.10.cloned.1.call-start = ((), (), s32[]{:S(2)}) async-start(), calls=%async_computation.6 | async-start | bytes 327680 | tf_op jit(solution)/shard_map/reduce_scatter | solution.py:67
  24.7 51.5 %reduce-scatter.12.cloned.1.call-start = ((), (), s32[]{:S(2)}) async-start(), calls=%async_computation.7 | async-start | bytes 327680 | tf_op jit(solution)/shard_map/reduce_scatter | solution.py:68
  27.0 76.3 %reduce-scatter.14.cloned.1.call-start = ((), (), s32[]{:S(2)}) async-start(), calls=%async_computation.8 | async-start | bytes 327680 | tf_op jit(solution)/shard_map/reduce_scatter | solution.py:69
  29.3 101.0 %reduce-scatter.8.cloned.1.call-start = ((), (), s32[]{:S(2)}) async-start(), calls=%async_computation.5 | async-start | bytes 327680 | tf_op jit(solution)/shard_map/reduce_scatter | solution.py:66
  31.7 185.4 %all-reduce.4.cloned.1.call-start = ((), (), s32[]{:S(2)}) async-start(), calls=%async_computation.9 | async-start | bytes 1048576 | tf_op jit(solution)/shard_map/psum | solution.py:88
  139.8 3.4 %copy-start.1 = (f32[32,4,128,128]{3,2,1,0:T(8,128)}, f32[32,4,128,128]{3,2,1,0:T(8,128)S(1)}, u32[]{:S(2)}) copy-start(f32[32,4,128,128]{3,2,1,0:T(8,128)S(1)} %multiply_add_fusion) | copy-start | bytes 25165828
  139.8 10.8 %copy-start.5 = (f32[128]{0:T(128)S(1)}, f32[128]{0:T(128)}, u32[]{:S(2)}) copy-start(f32[128]{0:T(128)} %param.22) | copy-start | bytes 1540
  139.9 19.4 %copy-start.2 = (bf16[512,1024]{1,0:T(8,128)(2,1)S(1)}, bf16[512,1024]{1,0:T(8,128)(2,1)}, u32[]{:S(2)}) copy-start(bf16[512,1024]{1,0:T(8,128)(2,1)} %param.23) | copy-start | bytes 3145732
  139.9 78.4 %copy-start.3 = (f32[1024]{0:T(1024)S(1)}, f32[1024]{0:T(1024)}, u32[]{:S(2)}) copy-start(f32[1024]{0:T(1024)} %param.24) | copy-start | bytes 12292
  160.4 109.6 %all-reduce.6.cloned.1.call-start = ((), (), s32[]{:S(2)}) async-start(), calls=%async_computation.11 | async-start | bytes 1376256 | tf_op jit(solution)/shard_map/psum | solution.py:25
  223.4 81.2 %reduce-scatter.16.cloned.1.call-start = ((), (), s32[]{:S(2)}) async-start(), calls=%async_computation.10 | async-start | bytes 294912
Sparse Core Ops, SparseCore 0:
  24.8 24.1 reduce-scatter.9
  51.7 24.3 reduce-scatter.11
  78.9 24.3 reduce-scatter.13
  105.9 24.3 reduce-scatter.7
  160.5 56.5 all-reduce.3
  223.5 46.4 all-reduce.5
  273.7 30.7 reduce-scatter.15
where the time goes:
time: 314 us; the launch traced here: 313 us
  waiting for transfers between devices  212 us (68%)
  blocking collectives  43.7 us (14%)
  matrix products  25.2 us (8%)
  between operations  14.3 us (5%)
  other arithmetic  12.3 us (4%)
  local copies, waits for them, and re-layouts  5.22 us (2%)
    psum x1, waiting for transfers between devices, body(): mixed = lax.psum(terms, 'tp')  56.7 us
    psum x1, waiting for transfers between devices, channel_mix(): lax.psum(upper.astype(jnp.bfloat16), 'kv').astype(jnp.float32)  36.4 us
    unnamed x8, waiting for transfers between devices  31.1 us
    reduce_scatter x1, waiting for transfers between devices, body(): lax.psum_scatter(part_gate, 'kv', scatter_dimension=0, tiled=True)  27.2 us
    reduce_scatter x1, waiting for transfers between devices, body(): lax.psum_scatter(part_value, 'kv', scatter_dimension=0, tiled=True)  27.1 us
    reduce_scatter x1, waiting for transfers between devices, body(): lax.psum_scatter(part_query, 'kv', scatter_dimension=0, tiled=True)  27 us
    all_gather x1, blocking collectives, body(): rows = lax.all_gather(residual, 'tp', axis=1, tiled=True)  15.1 us
    psum x1, blocking collectives, channel_mix(): whole_total = lax.psum(squares, 'kv')  10.2 us
  transfers between devices with their start and end apart: 7, of which 7 were waited for; matrix products, arithmetic and copies ran while one was open for 2% of the time, Pallas kernels for 0%

commit v1 on v0

--- a/solution.py
+++ b/solution.py
@@ -85,7 +85,7 @@
         .astype(jnp.bfloat16)
     )
     terms = project_row(w_mix_out, lax.all_gather(normed, "kv", axis=0, tiled=True))
-    mixed = lax.psum(terms, "tp")
+    mixed = jnp.sum(lax.all_gather(terms, "tp"), axis=0)
     after_mix = (rows_float + mixed).astype(jnp.bfloat16)
     layer_out = channel_mix(after_mix, ffn_gain, w_gate, w_up, w_down)
     return (layer_out, updated)

time: 314 us -> 302 us (0.962)
  waiting for transfers between devices: 212 us -> 203 us
  local copies, waits for them, and re-layouts: 5.22 us -> 1.87 us
    psum x1 -> x0, waiting for transfers between devices: 56.7 us -> none  [body(): mixed = lax.psum(terms, 'tp')]
    all_gather x0 -> x1, waiting for transfers between devices: none -> 47 us  [body(): mixed = jnp.sum(lax.all_gather(terms, 'tp'), axis=0)]
    reduce_sum x0 -> x1, other arithmetic: none -> 3.4 us  [body(): mixed = jnp.sum(lax.all_gather(terms, 'tp'), axis=0)]
    unnamed x17 -> x21, local copies, waits for them, and re-layouts: 5.09 us -> 1.75 us
where the time goes in v1:
time: 302 us; the launch traced here: 301 us
  waiting for transfers between devices  203 us (67%)
  blocking collectives  43.7 us (14%)
  matrix products  23.4 us (8%)
  other arithmetic  15.2 us (5%)
  between operations  14.4 us (5%)
    all_gather x1, waiting for transfers between devices, body(): mixed = jnp.sum(lax.all_gather(terms, 'tp'), axis=0)  47 us
    psum x1, waiting for transfers between devices, channel_mix(): lax.psum(upper.astype(jnp.bfloat16), 'kv').astype(jnp.float32)  36.1 us
    unnamed x8, waiting for transfers between devices  31.1 us
    reduce_scatter x1, waiting for transfers between devices, body(): lax.psum_scatter(part_gate, 'kv', scatter_dimension=0, tiled=True)  27.1 us
    reduce_scatter x1, waiting for transfers between devices, body(): lax.psum_scatter(part_value, 'kv', scatter_dimension=0, tiled=True)  27.1 us
    reduce_scatter x1, waiting for transfers between devices, body(): lax.psum_scatter(part_query, 'kv', scatter_dimension=0, tiled=True)  27 us
    all_gather x1, blocking collectives, body(): rows = lax.all_gather(residual, 'tp', axis=1, tiled=True)  15.1 us
    psum x1, blocking collectives, channel_mix(): whole_total = lax.psum(squares, 'kv')  10.2 us
  transfers between devices with their start and end apart: 7, of which 7 were waited for; matrix products, arithmetic and copies ran while one was open for 2% of the time, Pallas kernels for 0%

profile of v1, /device:TPU:0, one launch (start us, length us, event | category | flops | bytes accessed | tf_op | source)
XLA Modules:
  0.0 301.3 jit_solution(16050818123356955633)
XLA Ops:
  7.2 0.0 copy-start
  7.2 0.0 copy-start.4
  7.2 0.0 copy-start.6
  7.2 0.0 reduce-scatter.10.cloned.1.call-start
  7.2 15.1 %all_gather.12 = bf16[128,1024]{1,0:T(8,128)(2,1)S(1)} all-gather(bf16[128,128]{1,0:T(8,128)(2,1)} %param.14), channel_id=1, replica_groups=mesh['kv'=4,'tp'=8] {'tp'}, dimensions={1}, use_global_device_ids=true | all-gather | bytes 294912 | tf_op jit(solution)/shard_map/all_gather | solution.py:55
  22.4 2.3 fusion.10
  24.7 0.0 reduce-scatter.10.cloned.1.call-update
  24.7 0.0 reduce-scatter.12.cloned.1.call-start
  24.7 2.2 fusion.8
  27.0 0.0 reduce-scatter.12.cloned.1.call-update
  27.0 0.0 reduce-scatter.14.cloned.1.call-start
  27.1 2.3 fusion.6
  29.3 0.0 reduce-scatter.14.cloned.1.call-update
  29.3 0.0 reduce-scatter.8.cloned.1.call-start
  29.4 0.0 copy-done.4
  29.4 2.2 fusion.12
  31.6 0.0 reduce-scatter.8.cloned.1.call-update
  31.7 0.0 all-gather.3.cloned.1.call-start
  31.7 0.1 fusion.1
  31.8 9.9 %psum.28 = f32[128]{0:T(128)S(1)} all-reduce(f32[128]{0:T(128)S(1)} %fusion.1), channel_id=1, replica_groups=mesh['kv'=4,'tp'=8] {'kv'}, use_global_device_ids=true, to_apply=%region_2.0 | all-reduce | flops 128 | bytes 1024 | tf_op jit(solution)/shard_map/psum | solution.py:63
  41.8 0.1 add_rsqrt_fusion.2
  41.8 0.0 copy-done.6
  41.8 7.1 %reduce-scatter.10.cloned.1.call-done = f32[32,512]{1,0:T(8,128)} async-done(((f32[128,512]{1,0:T(8,128)}), f32[32,512]{1,0:T(8,128)}) %reduce-scatter.10.cloned.1.call-update) | async-done | bytes 65552 | tf_op jit(solution)/shard_map/reduce_scatter | solution.py:67
  49.0 27.1 %reduce-scatter.12.cloned.1.call-done = f32[32,512]{1,0:T(8,128)} async-done(((f32[128,512]{1,0:T(8,128)}), f32[32,512]{1,0:T(8,128)}) %reduce-scatter.12.cloned.1.call-update) | async-done | bytes 65552 | tf_op jit(solution)/shard_map/reduce_scatter | solution.py:68
  76.1 27.1 %reduce-scatter.14.cloned.1.call-done = f32[32,512]{1,0:T(8,128)} async-done(((f32[128,512]{1,0:T(8,128)}), f32[32,512]{1,0:T(8,128)}) %reduce-scatter.14.cloned.1.call-update) | async-done | bytes 65552 | tf_op jit(solution)/shard_map/reduce_scatter | solution.py:69
  103.2 27.0 %reduce-scatter.8.cloned.1.call-done = f32[32,512]{1,0:T(8,128)} async-done(((f32[128,512]{1,0:T(8,128)}), f32[32,512]{1,0:T(8,128)}) %reduce-scatter.8.cloned.1.call-update) | async-done | bytes 65552 | tf_op jit(solution)/shard_map/reduce_scatter | solution.py:66
  130.2 1.0 add_divide_fusion.1
  131.5 8.2 %multiply_add_fusion = f32[32,4,128,128]{3,2,1,0:T(8,128)S(1)} fusion(f32[32,4,128,128]{3,2,1,0:T(8,128)} %param.21, f32[32,4,128]{2,1,0:T(4,128)S(1)} %mul.164, f32[32,4,128]{2,1,0:T(4,128)S(1)} %bitcast.37, f32[32,4,128]{2,1,0:T(4,128)S(1)} %bitcast.36), kind=kLoop, calls=%fused_computation | loop fusion | flops 6291456 | bytes 16973824 | tf_op jit(solution)/shard_map/add | solution.py:78
  139.7 0.0 copy-start.1
  139.8 0.0 copy-start.7
  139.8 0.0 copy-start.3
  139.8 7.2 %fusion.18 = f32[32,4,1,128]{3,2,1,0:T(1,128)S(1)} fusion(f32[32,4,128,1]{2,3,1,0:T(1,128)S(1)} %bitcast.35, f32[32,4,128,128]{3,2,1,0:T(8,128)S(1)} %multiply_add_fusion), kind=kOutput, calls=%fused_computation.39 | convolution fusion | flops 25165824 | bytes 8519680 | tf_op jit(solution)/shard_map/shc,shce->she/dot_general | solution.py:79
  147.0 0.0 copy-done.1
  147.0 0.1 multiply_reduce_fusion.1
  147.2 0.0 copy-done.7
  147.2 0.1 fusion.15
  147.3 0.0 copy-start.5
  147.3 8.5 %all_gather.13 = bf16[128,512]{1,0:T(8,128)(2,1)S(1)} all-gather(bf16[32,512]{1,0:T(8,128)(2,1)S(1)} %bitcast.40), channel_id=1, replica_groups=mesh['kv'=4,'tp'=8] {'kv'}, dimensions={0}, use_global_device_ids=true | all-gather | bytes 163840 | tf_op jit(solution)/shard_map/all_gather | solution.py:87
  155.8 0.0 copy-done.3
  155.8 1.1 fusion.19
  156.9 0.0 all-gather.3.cloned.1.call-update
  157.0 0.0 all-reduce.3.cloned.1.call-start
  157.0 47.0 %all-gather.3.cloned.1.call-done = f32[1024,1024]{1,0:T(8,128)} async-done(((f32[128,1024]{1,0:T(8,128)}), f32[1024,1024]{1,0:T(8,128)}) %all-gather.3.cloned.1.call-update) | async-done | bytes 4194320 | tf_op jit(solution)/shard_map/all_gather | solution.py:88
  204.0 3.4 %reduce_sum.38 = f32[128,1024]{1,0:T(8,128)} reduce(f32[8,128,1024]{2,1,0:T(8,128)} %bitcast.31, f32[]{:T(128)} %constant.11.clone.1), dimensions={0}, to_apply=%region_7.8 | reduce | flops 917504 | bytes 4718596 | tf_op jit(solution)/shard_map/reduce_sum | solution.py:88
  207.4 0.0 copy-start.2
  207.4 1.3 multiply_reduce_fusion
  208.7 0.0 copy-done
  208.7 0.0 copy-done.5
  208.7 1.6 convolution_convert_fusion
  210.4 0.0 copy-done.2
  210.4 1.6 convolution_convert_fusion.1
  212.0 0.0 all-reduce.3.cloned.1.call-update
  212.0 0.0 reduce-scatter.16.cloned.1.call-start
  212.1 10.2 %psum.30 = f32[128]{0:T(128)S(1)} all-reduce(f32[128]{0:T(128)S(1)} %get-tuple-element.4), channel_id=1, replica_groups=mesh['kv'=4,'tp'=8] {'kv'}, use_global_device_ids=true, to_apply=%region_10.11 | all-reduce | flops 128 | bytes 1024 | tf_op jit(solution)/shard_map/psum | solution.py:22
  222.2 36.1 %all-reduce.3.cloned.1.call-done = (bf16[128,1344]{0,1:T(8,128)(2,1)}, bf16[128,1344]{0,1:T(8,128)(2,1)}) async-done(((bf16[128,1344]{0,1:T(8,128)(2,1)}, bf16[128,1344]{0,1:T(8,128)(2,1)}), (bf16[128,1344]{0,1:T(8,128)(2,1)}, bf16[128,1344]{0,1:T(8,128)(2,1)})) %all-reduce.3.cloned.1.call-update) | async-done | bytes 688144 | tf_op jit(solution)/shard_map/psum | solution.py:25
  258.4 2.8 convolution_convert_fusion.2
  261.1 0.8 copy.18
  262.0 0.0 reduce-scatter.16.cloned.1.call-update
  262.0 31.0 %reduce-scatter.16.cloned.1.call-done = bf16[128,128]{1,0:T(8,128)(2,1)} async-done(((bf16[1024,128]{1,0:T(8,128)(2,1)}), bf16[128,128]{1,0:T(8,128)(2,1)}) %reduce-scatter.16.cloned.1.call-update) | async-done | bytes 32784
  293.0 0.9 copy.19
  293.9 0.6 add_convert_fusion
  (13 shorter events, 0.2 us)
Async XLA Ops:
  7.2 201.6 %copy-start = (bf16[1024,1344]{0,1:T(8,128)(2,1)S(1)}, bf16[1024,1344]{0,1:T(8,128)(2,1)}, u32[]{:S(2)}) copy-start(bf16[1024,1344]{0,1:T(8,128)(2,1)} %param.26) | copy-start | bytes 8257540
  7.2 22.2 %copy-start.4 = (f32[1024]{0:T(1024)S(1)}, f32[1024]{0:T(1024)}, u32[]{:S(2)}) copy-start(f32[1024]{0:T(1024)} %param.15) | copy-start | bytes 12292
  7.2 34.7 %copy-start.6 = (f32[512]{0:T(512)S(1)}, f32[512]{0:T(512)}, u32[]{:S(2)}) copy-start(f32[512]{0:T(512)} %param.20) | copy-start | bytes 6148
  7.2 41.8 %reduce-scatter.10.cloned.1.call-start = ((), (), s32[]{:S(2)}) async-start(), calls=%async_computation.6 | async-start | bytes 327680 | tf_op jit(solution)/shard_map/reduce_scatter | solution.py:67
  24.7 51.4 %reduce-scatter.12.cloned.1.call-start = ((), (), s32[]{:S(2)}) async-start(), calls=%async_computation.7 | async-start | bytes 327680 | tf_op jit(solution)/shard_map/reduce_scatter | solution.py:68
  27.0 76.2 %reduce-scatter.14.cloned.1.call-start = ((), (), s32[]{:S(2)}) async-start(), calls=%async_computation.8 | async-start | bytes 327680 | tf_op jit(solution)/shard_map/reduce_scatter | solution.py:69
  29.3 100.9 %reduce-scatter.8.cloned.1.call-start = ((), (), s32[]{:S(2)}) async-start(), calls=%async_computation.5 | async-start | bytes 327680 | tf_op jit(solution)/shard_map/reduce_scatter | solution.py:66
  31.7 172.3 %all-gather.3.cloned.1.call-start = ((), (), s32[]{:S(2)}) async-start(), calls=%async_computation.9 | async-start | bytes 4718592 | tf_op jit(solution)/shard_map/all_gather | solution.py:88
  139.7 7.3 %copy-start.1 = (f32[32,4,128,128]{3,2,1,0:T(8,128)}, f32[32,4,128,128]{3,2,1,0:T(8,128)S(1)}, u32[]{:S(2)}) copy-start(f32[32,4,128,128]{3,2,1,0:T(8,128)S(1)} %multiply_add_fusion) | copy-start | bytes 25165828
  139.8 7.4 %copy-start.7 = (f32[128]{0:T(128)S(1)}, f32[128]{0:T(128)}, u32[]{:S(2)}) copy-start(f32[128]{0:T(128)} %param.22) | copy-start | bytes 1540
  139.8 16.1 %copy-start.3 = (bf16[512,1024]{1,0:T(8,128)(2,1)S(1)}, bf16[512,1024]{1,0:T(8,128)(2,1)}, u32[]{:S(2)}) copy-start(bf16[512,1024]{1,0:T(8,128)(2,1)} %param.23) | copy-start | bytes 3145732
  147.3 61.4 %copy-start.5 = (f32[1024]{0:T(1024)S(1)}, f32[1024]{0:T(1024)}, u32[]{:S(2)}) copy-start(f32[1024]{0:T(1024)} %param.24) | copy-start | bytes 12292
  157.0 101.4 %all-reduce.3.cloned.1.call-start = ((), (), s32[]{:S(2)}) async-start(), calls=%async_computation.11 | async-start | bytes 1376256 | tf_op jit(solution)/shard_map/psum | solution.py:25
  207.4 3.0 copy-start.2
  212.0 81.0 %reduce-scatter.16.cloned.1.call-start = ((), (), s32[]{:S(2)}) async-start(), calls=%async_computation.10 | async-start | bytes 294912
Sparse Core Ops, SparseCore 0:
  24.8 24.1 reduce-scatter.9
  51.8 24.3 reduce-scatter.11
  78.9 24.3 reduce-scatter.13
  105.8 24.3 reduce-scatter.7
  157.1 46.8 all-gather.2
  212.1 46.2 all-reduce.2
  262.1 30.8 reduce-scatter.15
